TPU v7x, 32 devices: a whole 2x2x4 slice. The times are simulated.
32 devices in a mesh: grp: 2 (over y), ra: 4 (over z), cb: 4 (over x, core).
Axes of the slice: x: 2, y: 2, z: 4, core: 2. Of those that a mesh axis runs over, the one named last changes fastest.
Arguments:
- tokens: bfloat16 [512, 4096], P('grp', 'cb'), parts along dimension 0, may hold values from -50 to 50
- norm_gains: float32 [3, 4096], P(None, 'cb'), may hold values from 0.1 to 1.9
- gate_weight: float32 [2, 4096, 11264], P(None, 'cb', 'ra'), may hold values from -0.09375 to 0.09375
- value_weight: float32 [2, 4096, 11264], P(None, 'cb', 'ra'), may hold values from -0.09375 to 0.09375
- gate_scale: float32 [2, 11264], P(None, 'ra'), may hold values from 0.3 to 3
- value_scale: float32 [2, 11264], P(None, 'ra'), may hold values from 0.3 to 3
- conv_gate: float32 [2, 3, 11264], P(None, None, 'ra'), may hold values from -3 to 3
- conv_value: float32 [2, 3, 11264], P(None, None, 'ra'), may hold values from -3 to 3
- down_weight: float32 [2, 11264, 4096], P(None, 'ra', 'cb'), may hold values from -0.07537784 to 0.07537784
- down_scale: float32 [2, 4096], P(None, 'cb'), may hold values from 0.3 to 3
Outputs:
- normed_out: bfloat16 [512, 4096], P('grp', 'cb'), parts along dimension 0
There are 2 independent parts, one for each index of `grp`. A program takes and returns all parts, laid end to end along the dimension named above; an argument that names none is the same for every part. Nothing has to cross between parts.
All inputs are finite; a program needn't handle non-finite values.
Results may differ from a plain program's by a relative error of at most 0.012.
The roundings to bfloat16 on the way count: a program that leaves them out, or rounds other values in their place, can miss the bound.
Values may be sent and summed in bfloat16 or wider, within the bound.
A program may use at most 192 MiB of HBM per device.

v0:
```python
import jax
import jax.numpy as jnp
from jax import lax
from jax.sharding import PartitionSpec as P

epsilon = 1e-06
residual_weight = 0.5


def causal_taps(projected, tap_weights):
    tap_count = tap_weights.shape[0]
    row_count = projected.shape[0]
    padded = jnp.pad(projected, ((tap_count - 1, 0), (0, 0)))
    result = jnp.zeros_like(projected)
    for tap_idx in range(tap_count):
        result = result + padded[tap_idx : tap_idx + row_count] * tap_weights[tap_idx]
    return result


def row_inverse(state_wide, model_width):
    squares = lax.psum(jnp.sum(state_wide * state_wide, axis=1, keepdims=True), "cb")
    return lax.rsqrt(squares / model_width + epsilon)


def on_device(
    tokens,
    norm_gains,
    gate_weight,
    value_weight,
    gate_scale,
    value_scale,
    conv_gate,
    conv_value,
    down_weight,
    down_scale,
):
    model_width = lax.axis_size("cb") * tokens.shape[1]
    layer_count = gate_weight.shape[0]
    current = tokens
    for layer_idx in range(layer_count):
        state_wide = current.astype(jnp.float32)
        inverse = row_inverse(state_wide, model_width)
        scaled = (state_wide * norm_gains[layer_idx]).astype(jnp.bfloat16)
        gate_part = jnp.dot(
            scaled, gate_weight[layer_idx].astype(jnp.bfloat16), preferred_element_type=jnp.float32
        )
        value_part = jnp.dot(
            scaled, value_weight[layer_idx].astype(jnp.bfloat16), preferred_element_type=jnp.float32
        )
        gate_sum, value_sum = (
            lax.psum_scatter(gate_part, "cb", scatter_dimension=1, tiled=True),
            lax.psum_scatter(value_part, "cb", scatter_dimension=1, tiled=True),
        )
        share_cols = gate_sum.shape[1]
        first_col = lax.axis_index("cb") * share_cols
        gate_cols = lax.dynamic_slice_in_dim(gate_scale[layer_idx], first_col, share_cols, 0)
        value_cols = lax.dynamic_slice_in_dim(value_scale[layer_idx], first_col, share_cols, 0)
        gate_taps = lax.dynamic_slice_in_dim(conv_gate[layer_idx], first_col, share_cols, 1)
        value_taps = lax.dynamic_slice_in_dim(conv_value[layer_idx], first_col, share_cols, 1)
        gate_pre = inverse * gate_cols * gate_sum
        value_pre = inverse * value_cols * value_sum
        hidden = (
            jax.nn.gelu(causal_taps(gate_pre, gate_taps), approximate=True)
            * causal_taps(value_pre, value_taps)
        ).astype(jnp.bfloat16)
        hidden = lax.all_gather(hidden, "cb", axis=1, tiled=True)
        partial_value = jnp.dot(
            hidden, down_weight[layer_idx].astype(jnp.bfloat16), preferred_element_type=jnp.float32
        )
        down_total = lax.psum(partial_value, "ra")
        current = (residual_weight * state_wide + down_scale[layer_idx] * down_total).astype(
            jnp.bfloat16
        )
    state_wide = current.astype(jnp.float32)
    inverse = row_inverse(state_wide, model_width)
    return (state_wide * inverse * norm_gains[layer_count]).astype(jnp.bfloat16)


def solution(mesh):
    in_specs = (
        P("grp", "cb"),
        P(None, "cb"),
        P(None, "cb", "ra"),
        P(None, "cb", "ra"),
        P(None, "ra"),
        P(None, "ra"),
        P(None, None, "ra"),
        P(None, None, "ra"),
        P(None, "ra", "cb"),
        P(None, "cb"),
    )
    out_specs = P("grp", "cb")
    return jax.shard_map(
        on_device, mesh=mesh, in_specs=in_specs, out_specs=out_specs, check_vma=False
    )
```

profile of v0, /device:TPU:0, one launch (start us, length us, event | category | flops | bytes accessed | tf_op | source)
XLA Modules:
  0.0 362.3 jit_solution(13226815253919093914)
XLA Ops:
  6.5 0.0 reduce-scatter.5.cloned.1.call-start
  6.5 0.8 fusion.77
  7.4 0.0 copy-start.2
  7.4 8.6 %convert.12 = bf16[2,1024,2816]{2,1,0:T(8,128)(2,1)S(1)} convert(f32[2,1024,2816]{2,1,0:T(8,128)} %param.12) | non-fusion elementwise | flops 5767168 | bytes 34603008 | tf_op jit(solution)/shard_map/convert.5
  16.0 0.0 copy-start.1
  16.0 4.2 %copy-done.1 = bf16[2,1024,2816]{2,1,0:T(8,128)(2,1)} copy-done((bf16[2,1024,2816]{2,1,0:T(8,128)(2,1)}, bf16[2,1024,2816]{2,1,0:T(8,128)(2,1)S(1)}, u32[]{:S(2)}) %copy-start.1) | copy-done | bytes 11534360
  20.2 0.0 copy-done.2
  20.2 4.1 %fusion.5 = f32[256,2816]{0,1:T(8,128)} fusion(bf16[2,1024,2816]{2,1,0:T(8,128)(2,1)S(1)} %convert.12, bf16[256,1024]{1,0:T(8,128)(2,1)S(1)} %copy-done.2, f32[1024]{0:T(1024)S(1)} %bitcast.42), kind=kOutput, calls=%fused_computation.11 | convolution fusion | flops 1477181440 | bytes 9179136 | tf_op jit(solution)/shard_map/dot_general | solution.py:44
  24.3 0.0 reduce-scatter.5.cloned.1.call-update
  24.3 0.0 reduce-scatter.7.cloned.1.call-start
  24.4 8.6 %convert.13 = bf16[2,1024,2816]{2,1,0:T(8,128)(2,1)S(1)} convert(f32[2,1024,2816]{2,1,0:T(8,128)} %param.13) | non-fusion elementwise | flops 5767168 | bytes 34603008 | tf_op jit(solution)/shard_map/convert.4
  32.9 0.0 copy-start
  32.9 4.8 %copy-done = bf16[2,1024,2816]{2,1,0:T(8,128)(2,1)} copy-done((bf16[2,1024,2816]{2,1,0:T(8,128)(2,1)}, bf16[2,1024,2816]{2,1,0:T(8,128)(2,1)S(1)}, u32[]{:S(2)}) %copy-start) | copy-done | bytes 11534360
  37.7 0.0 copy-start.6
  37.8 0.0 copy-start.3
  37.8 4.0 %fusion.4 = f32[256,2816]{0,1:T(8,128)} fusion(bf16[2,1024,2816]{2,1,0:T(8,128)(2,1)S(1)} %convert.13, bf16[256,1024]{1,0:T(8,128)(2,1)S(1)} %copy-done.2, f32[1024]{0:T(1024)S(1)} %bitcast.43), kind=kOutput, calls=%fused_computation.9 | convolution fusion | flops 1477181440 | bytes 9179136 | tf_op jit(solution)/shard_map/dot_general | solution.py:47
  41.8 0.0 reduce-scatter.7.cloned.1.call-update
  41.8 0.0 all-gather.3.cloned.1.call-start
  41.8 0.0 copy-done.5
  41.9 0.0 copy-done.6
  41.9 0.1 fusion.55
  42.0 0.2 fusion.11
  42.2 9.0 %psum.35 = f32[256,1]{0,1:T(1,128)S(1)} all-reduce(f32[256,1]{0,1:T(1,128)S(1)} %bitcast.39), channel_id=1, replica_groups=mesh['grp'=2,'ra'=4,'cb'=4] {'cb'}, use_global_device_ids=true, to_apply=%region_1.0 | all-reduce | flops 256 | bytes 2048 | tf_op jit(solution)/shard_map/psum | solution.py:21
  51.2 0.0 copy-done.3
  51.2 0.1 fusion.73
  51.3 0.0 copy-done.4
  51.3 0.1 fusion.74
  51.3 0.1 fusion.63
  51.5 12.1 %reduce-scatter.5.cloned.1.call-done = f32[256,704]{0,1:T(8,128)} async-done(((f32[256,2816]{0,1:T(8,128)}), f32[256,704]{0,1:T(8,128)}) %reduce-scatter.5.cloned.1.call-update) | async-done | bytes 720912 | tf_op jit(solution)/shard_map/reduce_scatter | solution.py:51
  63.5 38.8 %reduce-scatter.7.cloned.1.call-done = f32[256,704]{0,1:T(8,128)} async-done(((f32[256,2816]{0,1:T(8,128)}), f32[256,704]{0,1:T(8,128)}) %reduce-scatter.7.cloned.1.call-update) | async-done | bytes 720912 | tf_op jit(solution)/shard_map/reduce_scatter | solution.py:52
  102.3 1.6 multiply_multiply_fusion.4
  103.9 2.2 fusion.25
  106.1 0.0 all-gather.3.cloned.1.call-update
  106.1 0.0 all-reduce.7.cloned.1.call-start
  106.2 12.6 %convert.14 = bf16[2,2816,1024]{2,1,0:T(8,128)(2,1)} convert(f32[2,2816,1024]{2,1,0:T(8,128)} %param.18) | non-fusion elementwise | flops 5767168 | bytes 34603008 | tf_op jit(solution)/shard_map/convert.3
  118.8 6.4 %all-gather.3.cloned.1.call-done = bf16[256,2816]{0,1:T(8,128)(2,1)} async-done(((bf16[256,704]{0,1:T(8,128)(2,1)}), bf16[256,2816]{0,1:T(8,128)(2,1)}) %all-gather.3.cloned.1.call-update) | async-done | bytes 1441808 | tf_op jit(solution)/shard_map/all_gather | solution.py:66
  125.2 5.8 %fusion.3 = f32[256,1024]{1,0:T(8,128)} fusion(bf16[256,2816]{0,1:T(8,128)(2,1)} %all-gather.3.cloned.1.call-done, bf16[2,2816,1024]{2,1,0:T(8,128)(2,1)} %convert.14), kind=kOutput, calls=%fused_computation.7 | convolution fusion | flops 1476395008 | bytes 8257536 | tf_op jit(solution)/shard_map/dot_general | solution.py:67
  130.9 0.0 all-reduce.7.cloned.1.call-update
  130.9 0.0 reduce-scatter.9.cloned.1.call-start
  131.0 0.0 copy-done.7
  131.0 52.0 %all-reduce.7.cloned.1.call-done = f32[256,1024]{1,0:T(8,128)} async-done(((f32[256,1024]{1,0:T(8,128)}), f32[256,1024]{1,0:T(8,128)}) %all-reduce.7.cloned.1.call-update) | async-done | bytes 1048592 | tf_op jit(solution)/shard_map/psum | solution.py:70
  183.0 1.5 fusion.15
  184.5 6.6 %fusion.2 = f32[256,2816]{0,1:T(8,128)} fusion(bf16[2,1024,2816]{2,1,0:T(8,128)(2,1)} %copy-done.1, bf16[256,1024]{1,0:T(8,128)(2,1)S(1)} %get-tuple-element.20, f32[1024]{0:T(1024)S(1)} %bitcast.40), kind=kOutput, calls=%fused_computation.5 | convolution fusion | flops 1477181440 | bytes 9179136 | tf_op jit(solution)/shard_map/dot_general | solution.py:44
  191.2 0.0 reduce-scatter.9.cloned.1.call-update
  191.2 0.2 reduce-scatter.11.cloned.1.call-start
  191.4 6.6 %fusion.1 = f32[256,2816]{0,1:T(8,128)} fusion(bf16[2,1024,2816]{2,1,0:T(8,128)(2,1)} %copy-done, bf16[256,1024]{1,0:T(8,128)(2,1)S(1)} %get-tuple-element.20, f32[1024]{0:T(1024)S(1)} %bitcast.41), kind=kOutput, calls=%fused_computation.3 | convolution fusion | flops 1477181440 | bytes 9179136 | tf_op jit(solution)/shard_map/dot_general | solution.py:47
  198.0 0.0 reduce-scatter.11.cloned.1.call-update
  198.1 0.0 all-gather.5.cloned.1.call-start
  198.1 0.1 fusion.59
  198.2 0.1 fusion.69
  198.3 6.8 %psum.37 = f32[256,1]{0,1:T(1,128)S(1)} all-reduce(f32[256,1]{0,1:T(1,128)S(1)} %bitcast.34), channel_id=1, replica_groups=mesh['grp'=2,'ra'=4,'cb'=4] {'cb'}, use_global_device_ids=true, to_apply=%region_6.7 | all-reduce | flops 256 | bytes 2048 | tf_op jit(solution)/shard_map/psum | solution.py:21
  205.2 21.6 %reduce-scatter.9.cloned.1.call-done = f32[256,704]{0,1:T(8,128)} async-done(((f32[256,2816]{0,1:T(8,128)}), f32[256,704]{0,1:T(8,128)}) %reduce-scatter.9.cloned.1.call-update) | async-done | bytes 720912 | tf_op jit(solution)/shard_map/reduce_scatter | solution.py:51
  226.8 38.6 %reduce-scatter.11.cloned.1.call-done = f32[256,704]{0,1:T(8,128)} async-done(((f32[256,2816]{0,1:T(8,128)}), f32[256,704]{0,1:T(8,128)}) %reduce-scatter.11.cloned.1.call-update) | async-done | bytes 720912 | tf_op jit(solution)/shard_map/reduce_scatter | solution.py:52
  265.4 1.6 multiply_multiply_fusion.2
  267.0 2.2 fusion.34
  269.2 0.0 all-gather.5.cloned.1.call-update
  269.2 0.0 all-reduce.9.cloned.1.call-start
  269.3 19.0 %all-gather.5.cloned.1.call-done = bf16[256,2816]{0,1:T(8,128)(2,1)} async-done(((bf16[256,704]{0,1:T(8,128)(2,1)}), bf16[256,2816]{0,1:T(8,128)(2,1)}) %all-gather.5.cloned.1.call-update) | async-done | bytes 1441808 | tf_op jit(solution)/shard_map/all_gather | solution.py:66
  288.3 5.7 %fusion = f32[256,1024]{1,0:T(8,128)} fusion(bf16[256,2816]{0,1:T(8,128)(2,1)} %all-gather.5.cloned.1.call-done, bf16[2,2816,1024]{2,1,0:T(8,128)(2,1)} %convert.14), kind=kOutput, calls=%fused_computation.1 | convolution fusion | flops 1476395008 | bytes 8257536 | tf_op jit(solution)/shard_map/dot_general | solution.py:67
  294.0 0.0 all-reduce.9.cloned.1.call-update
  294.0 52.1 %all-reduce.9.cloned.1.call-done = f32[256,1024]{1,0:T(8,128)} async-done(((f32[256,1024]{1,0:T(8,128)}), f32[256,1024]{1,0:T(8,128)}) %all-reduce.9.cloned.1.call-update) | async-done | bytes 1048592 | tf_op jit(solution)/shard_map/psum | solution.py:70
  346.1 1.5 fusion.6
  347.6 6.8 %psum.39 = f32[256,1]{0,1:T(1,128)S(1)} all-reduce(f32[256,1]{0,1:T(1,128)S(1)} %bitcast.37), channel_id=1, replica_groups=mesh['grp'=2,'ra'=4,'cb'=4] {'cb'}, use_global_device_ids=true, to_apply=%region_11.12 | all-reduce | flops 256 | bytes 2048 | tf_op jit(solution)/shard_map/psum | solution.py:21
  354.5 1.0 fusion.8
  (9 shorter events, 0.1 us)
Async XLA Ops:
  6.5 57.0 %reduce-scatter.5.cloned.1.call-start = ((), (), s32[]{:S(2)}) async-start(), calls=%async_computation.4 | async-start | bytes 3604480 | tf_op jit(solution)/shard_map/reduce_scatter | solution.py:51
  7.4 12.8 %copy-start.2 = (bf16[256,1024]{1,0:T(8,128)(2,1)S(1)}, bf16[256,1024]{1,0:T(8,128)(2,1)}, u32[]{:S(2)}) copy-start(bf16[256,1024]{1,0:T(8,128)(2,1)} %param.10) | copy-start | bytes 1572868
  16.0 4.2 %copy-start.1 = (bf16[2,1024,2816]{2,1,0:T(8,128)(2,1)}, bf16[2,1024,2816]{2,1,0:T(8,128)(2,1)S(1)}, u32[]{:S(2)}) copy-start(bf16[2,1024,2816]{2,1,0:T(8,128)(2,1)S(1)} %convert.12) | copy-start | bytes 34603012
  24.3 78.0 %reduce-scatter.7.cloned.1.call-start = ((), (), s32[]{:S(2)}) async-start(), calls=%async_computation.5 | async-start | bytes 3604480 | tf_op jit(solution)/shard_map/reduce_scatter | solution.py:52
  32.9 4.8 %copy-start = (bf16[2,1024,2816]{2,1,0:T(8,128)(2,1)}, bf16[2,1024,2816]{2,1,0:T(8,128)(2,1)S(1)}, u32[]{:S(2)}) copy-start(bf16[2,1024,2816]{2,1,0:T(8,128)(2,1)S(1)} %convert.13) | copy-start | bytes 34603012
  37.7 4.1 %copy-start.5 = (f32[2,2816]{1,0:T(2,128)S(1)}, f32[2,2816]{1,0:T(2,128)}, u32[]{:S(2)}) copy-start(f32[2,2816]{1,0:T(2,128)} %param.14) | copy-start | bytes 67588
  37.7 4.1 %copy-start.6 = (f32[2,2816]{1,0:T(2,128)S(1)}, f32[2,2816]{1,0:T(2,128)}, u32[]{:S(2)}) copy-start(f32[2,2816]{1,0:T(2,128)} %param.15) | copy-start | bytes 67588
  37.8 13.5 %copy-start.3 = (f32[2,3,2816]{2,0,1:T(2,128)S(1)}, f32[2,3,2816]{2,0,1:T(2,128)}, u32[]{:S(2)}) copy-start(f32[2,3,2816]{2,0,1:T(2,128)} %param.16) | copy-start | bytes 202756
  37.8 13.5 %copy-start.4 = (f32[2,3,2816]{2,0,1:T(2,128)S(1)}, f32[2,3,2816]{2,0,1:T(2,128)}, u32[]{:S(2)}) copy-start(f32[2,3,2816]{2,0,1:T(2,128)} %param.17) | copy-start | bytes 202756
  41.8 83.4 %all-gather.3.cloned.1.call-start = ((), (), s32[]{:S(2)}) async-start(), calls=%async_computation.6 | async-start | bytes 1802240 | tf_op jit(solution)/shard_map/all_gather | solution.py:66
  106.1 76.9 %all-reduce.7.cloned.1.call-start = ((), (), s32[]{:S(2)}) async-start(), calls=%async_computation.7 | async-start | bytes 2097152 | tf_op jit(solution)/shard_map/psum | solution.py:70
  118.8 12.2 %copy-start.7 = (f32[2,1024]{1,0:T(2,128)S(1)}, f32[2,1024]{1,0:T(2,128)}, u32[]{:S(2)}) copy-start(f32[2,1024]{1,0:T(2,128)} %param.19) | copy-start | bytes 24580
  130.9 95.8 %reduce-scatter.9.cloned.1.call-start = ((), (), s32[]{:S(2)}) async-start(), calls=%async_computation.8 | async-start | bytes 3604480 | tf_op jit(solution)/shard_map/reduce_scatter | solution.py:51
  191.2 74.2 %reduce-scatter.11.cloned.1.call-start = ((), (), s32[]{:S(2)}) async-start(), calls=%async_computation.9 | async-start | bytes 3604480 | tf_op jit(solution)/shard_map/reduce_scatter | solution.py:52
  198.1 90.2 %all-gather.5.cloned.1.call-start = ((), (), s32[]{:S(2)}) async-start(), calls=%async_computation.10 | async-start | bytes 1802240 | tf_op jit(solution)/shard_map/all_gather | solution.py:66
  269.2 76.9 %all-reduce.9.cloned.1.call-start = ((), (), s32[]{:S(2)}) async-start(), calls=%async_computation.11 | async-start | bytes 2097152 | tf_op jit(solution)/shard_map/psum | solution.py:70
Sparse Core Ops, SparseCore 0:
  24.4 39.0 reduce-scatter.4
  66.1 36.1 reduce-scatter.6
  106.2 18.8 all-gather.2
  131.1 51.8 all-reduce.6
  191.3 35.4 reduce-scatter.8
  229.2 36.1 reduce-scatter.10
  269.3 18.8 all-gather.4
  294.1 51.8 all-reduce.8
where the time goes:
time: 363 us; the launch traced here: 362 us
  waiting for transfers between devices  241 us (66%)
  other arithmetic  41.6 us (11%)
  matrix products  32.8 us (9%)
  blocking collectives  22.7 us (6%)
  between operations  13.7 us (4%)
  local copies, waits for them, and re-layouts  10.5 us (3%)
    psum x2, waiting for transfers between devices, on_device(): down_total = lax.psum(partial_value, 'ra')  104 us
    reduce_scatter x2, waiting for transfers between devices, on_device(): lax.psum_scatter(value_part, 'cb', scatter_dimension=1, tiled=True)  77.4 us
    reduce_scatter x2, waiting for transfers between devices, on_device(): lax.psum_scatter(gate_part, 'cb', scatter_dimension=1, tiled=True)  33.6 us
    another operation x3, other arithmetic  29.8 us
    all_gather x2, waiting for transfers between devices, on_device(): hidden = lax.all_gather(hidden, 'cb', axis=1, tiled=True)  25.4 us
    psum x3, blocking collectives, row_inverse(): lax.psum(jnp.sum(state_wide * state_wide, axis=1, keepdims=True), 'cb')  22.7 us
    dot_general x2, matrix products, on_device(): jnp.dot(hidden, down_weight[layer_idx].astype(jnp.bfloat16), preferred_el...  11.5 us
    dot_general x2, matrix products, on_device(): jnp.dot(scaled, gate_weight[layer_idx].astype(jnp.bfloat16), preferred_el...  10.7 us
  transfers between devices with their start and end apart: 8, of which 8 were waited for; matrix products, arithmetic and copies ran while one was open for 9% of the time, Pallas kernels for 0%

commit v1 on v0

--- a/solution.py
+++ b/solution.py
@@ -67,7 +67,10 @@
         partial_value = jnp.dot(
             hidden, down_weight[layer_idx].astype(jnp.bfloat16), preferred_element_type=jnp.float32
         )
-        down_total = lax.psum(partial_value, "ra")
+        peers, down_total = (lax.axis_size("ra"), partial_value)
+        for far in [1 << k for k in range(peers.bit_length() - 1)]:
+            swap = [(i, i ^ far) for i in range(peers)]
+            down_total = down_total + lax.ppermute(down_total, "ra", swap)
         current = (residual_weight * state_wide + down_scale[layer_idx] * down_total).astype(
             jnp.bfloat16
         )

time: 363 us -> 401 us (1.10)
  waiting for transfers between devices: 241 us -> 277 us
  starting transfers between devices: 0.47 us -> 8.44 us
    ppermute x0 -> x4, waiting for transfers between devices: none -> 138 us  [on_device(): down_total = down_total + lax.ppermute(down_total, 'ra', swap)]
    psum x2 -> x0, waiting for transfers between devices: 104 us -> none  [on_device(): down_total = lax.psum(partial_value, 'ra')]
    ppermute x0 -> x4, starting transfers between devices: none -> 8.04 us  [on_device(): down_total = down_total + lax.ppermute(down_total, 'ra', swap)]
  transfers between devices with their start and end apart: 8 -> 10, of which waited for: 8 -> 10; matrix products, arithmetic and copies ran while one was open for 9% -> 8% of each run, Pallas kernels for 0% -> 0%
where the time goes in v1:
time: 401 us; the launch traced here: 400 us
  waiting for transfers between devices  277 us (69%)
  other arithmetic  39.6 us (10%)
  matrix products  30.9 us (8%)
  blocking collectives  20.5 us (5%)
  between operations  13.7 us (3%)
  local copies, waits for them, and re-layouts  10.5 us (3%)
  starting transfers between devices  8.44 us (2%)
    ppermute x4, waiting for transfers between devices, on_device(): down_total = down_total + lax.ppermute(down_total, 'ra', swap)  138 us
    reduce_scatter x2, waiting for transfers between devices, on_device(): lax.psum_scatter(value_part, 'cb', scatter_dimension=1, tiled=True)  77.4 us
    reduce_scatter x2, waiting for transfers between devices, on_device(): lax.psum_scatter(gate_part, 'cb', scatter_dimension=1, tiled=True)  35.4 us
    another operation x3, other arithmetic  29.8 us
    all_gather x2, waiting for transfers between devices, on_device(): hidden = lax.all_gather(hidden, 'cb', axis=1, tiled=True)  25.4 us
    psum x3, blocking collectives, row_inverse(): lax.psum(jnp.sum(state_wide * state_wide, axis=1, keepdims=True), 'cb')  20.5 us
    dot_general x2, matrix products, on_device(): jnp.dot(scaled, gate_weight[layer_idx].astype(jnp.bfloat16), preferred_el...  10.7 us
    dot_general x2, matrix products, on_device(): jnp.dot(scaled, value_weight[layer_idx].astype(jnp.bfloat16), preferred_e...  10.6 us
  transfers between devices with their start and end apart: 10, of which 10 were waited for; matrix products, arithmetic and copies ran while one was open for 8% of the time, Pallas kernels for 0%

profile of v1, /device:TPU:0, one launch (start us, length us, event | category | flops | bytes accessed | tf_op | source)
XLA Modules:
  0.0 400.3 jit_solution(9945474060387361138)
XLA Ops:
  6.5 0.0 reduce-scatter.5.cloned.1.call-start
  6.5 0.8 fusion.77
  7.4 0.0 copy-start.2
  7.4 8.6 %convert.12 = bf16[2,1024,2816]{2,1,0:T(8,128)(2,1)S(1)} convert(f32[2,1024,2816]{2,1,0:T(8,128)} %param.12) | non-fusion elementwise | flops 5767168 | bytes 34603008 | tf_op jit(solution)/shard_map/convert.5
  16.0 0.0 copy-start.1
  16.0 4.2 %copy-done.1 = bf16[2,1024,2816]{2,1,0:T(8,128)(2,1)} copy-done((bf16[2,1024,2816]{2,1,0:T(8,128)(2,1)}, bf16[2,1024,2816]{2,1,0:T(8,128)(2,1)S(1)}, u32[]{:S(2)}) %copy-start.1) | copy-done | bytes 11534360
  20.2 0.0 copy-done.2
  20.2 4.1 %fusion.5 = f32[256,2816]{0,1:T(8,128)} fusion(bf16[2,1024,2816]{2,1,0:T(8,128)(2,1)S(1)} %convert.12, bf16[256,1024]{1,0:T(8,128)(2,1)S(1)} %copy-done.2, f32[1024]{0:T(1024)S(1)} %bitcast.42), kind=kOutput, calls=%fused_computation.11 | convolution fusion | flops 1477181440 | bytes 9179136 | tf_op jit(solution)/shard_map/dot_general | solution.py:44
  24.3 0.0 reduce-scatter.5.cloned.1.call-update
  24.3 0.0 reduce-scatter.7.cloned.1.call-start
  24.4 8.6 %convert.13 = bf16[2,1024,2816]{2,1,0:T(8,128)(2,1)S(1)} convert(f32[2,1024,2816]{2,1,0:T(8,128)} %param.13) | non-fusion elementwise | flops 5767168 | bytes 34603008 | tf_op jit(solution)/shard_map/convert.4
  32.9 0.0 copy-start
  33.0 4.8 %copy-done = bf16[2,1024,2816]{2,1,0:T(8,128)(2,1)} copy-done((bf16[2,1024,2816]{2,1,0:T(8,128)(2,1)}, bf16[2,1024,2816]{2,1,0:T(8,128)(2,1)S(1)}, u32[]{:S(2)}) %copy-start) | copy-done | bytes 11534360
  37.8 4.0 fusion.4
  41.8 0.0 reduce-scatter.7.cloned.1.call-update
  41.8 0.0 all-gather.3.cloned.1.call-start
  41.8 0.0 copy-done.5
  41.9 0.0 copy-done.6
  41.9 0.1 fusion.55
  42.0 0.2 fusion.11
  42.2 9.0 %psum.21 = f32[256,1]{0,1:T(1,128)S(1)} all-reduce(f32[256,1]{0,1:T(1,128)S(1)} %bitcast.39), channel_id=1, replica_groups=mesh['grp'=2,'ra'=4,'cb'=4] {'cb'}, use_global_device_ids=true, to_apply=%region_1.0 | all-reduce | flops 256 | bytes 2048 | tf_op jit(solution)/shard_map/psum | solution.py:21
  51.2 0.0 copy-done.3
  51.2 0.1 fusion.73
  51.3 0.1 fusion.74
  51.3 0.1 fusion.63
  51.5 12.1 %reduce-scatter.5.cloned.1.call-done = f32[256,704]{0,1:T(8,128)} async-done(((f32[256,2816]{0,1:T(8,128)}), f32[256,704]{0,1:T(8,128)}) %reduce-scatter.5.cloned.1.call-update) | async-done | bytes 720912 | tf_op jit(solution)/shard_map/reduce_scatter | solution.py:51
  63.5 38.8 %reduce-scatter.7.cloned.1.call-done = f32[256,704]{0,1:T(8,128)} async-done(((f32[256,2816]{0,1:T(8,128)}), f32[256,704]{0,1:T(8,128)}) %reduce-scatter.7.cloned.1.call-update) | async-done | bytes 720912 | tf_op jit(solution)/shard_map/reduce_scatter | solution.py:52
  102.3 1.6 multiply_multiply_fusion.4
  103.9 2.2 fusion.25
  106.1 0.0 all-gather.3.cloned.1.call-update
  106.1 0.0 reduce-scatter.9.cloned.1.call-start
  106.2 12.6 %convert.14 = bf16[2,2816,1024]{2,1,0:T(8,128)(2,1)} convert(f32[2,2816,1024]{2,1,0:T(8,128)} %param.18) | non-fusion elementwise | flops 5767168 | bytes 34603008 | tf_op jit(solution)/shard_map/convert.3
  118.8 6.4 %all-gather.3.cloned.1.call-done = bf16[256,2816]{0,1:T(8,128)(2,1)} async-done(((bf16[256,704]{0,1:T(8,128)(2,1)}), bf16[256,2816]{0,1:T(8,128)(2,1)}) %all-gather.3.cloned.1.call-update) | async-done | bytes 1441808 | tf_op jit(solution)/shard_map/all_gather | solution.py:66
  125.2 4.8 %fusion.3 = f32[256,1024]{1,0:T(8,128)S(1)} fusion(bf16[256,2816]{0,1:T(8,128)(2,1)} %all-gather.3.cloned.1.call-done, bf16[2,2816,1024]{2,1,0:T(8,128)(2,1)} %convert.14), kind=kOutput, calls=%fused_computation.7 | convolution fusion | flops 1476395008 | bytes 8257536 | tf_op jit(solution)/shard_map/dot_general | solution.py:67
  129.9 1.5 collective-permute-start
  131.5 23.8 %collective-permute-done = f32[256,1024]{1,0:T(8,128)S(1)} collective-permute-done((f32[256,1024]{1,0:T(8,128)S(1)}, f32[256,1024]{1,0:T(8,128)S(1)}, u32[]{:S(2)}, u32[]{:S(2)}) %collective-permute-start) | collective-permute-done | bytes 1048608 | tf_op jit(solution)/shard_map/ppermute | solution.py:73
  155.3 0.2 add.103
  155.5 2.5 collective-permute-start.1
  157.9 45.4 %collective-permute-done.1 = f32[256,1024]{1,0:T(8,128)S(1)} collective-permute-done((f32[256,1024]{1,0:T(8,128)S(1)}, f32[256,1024]{1,0:T(8,128)S(1)}, u32[]{:S(2)}, u32[]{:S(2)}) %collective-permute-start.1) | collective-permute-done | bytes 1048608 | tf_op jit(solution)/shard_map/ppermute | solution.py:73
  203.3 0.4 fusion.15
  203.7 6.6 %fusion.2 = f32[256,2816]{0,1:T(8,128)} fusion(bf16[2,1024,2816]{2,1,0:T(8,128)(2,1)} %copy-done.1, bf16[256,1024]{1,0:T(8,128)(2,1)S(1)} %get-tuple-element.20, f32[1024]{0:T(1024)S(1)} %bitcast.40), kind=kOutput, calls=%fused_computation.5 | convolution fusion | flops 1477181440 | bytes 9179136 | tf_op jit(solution)/shard_map/dot_general | solution.py:44
  210.3 0.0 reduce-scatter.9.cloned.1.call-update
  210.3 0.2 reduce-scatter.11.cloned.1.call-start
  210.6 6.6 %fusion.1 = f32[256,2816]{0,1:T(8,128)} fusion(bf16[2,1024,2816]{2,1,0:T(8,128)(2,1)} %copy-done, bf16[256,1024]{1,0:T(8,128)(2,1)S(1)} %get-tuple-element.20, f32[1024]{0:T(1024)S(1)} %bitcast.41), kind=kOutput, calls=%fused_computation.3 | convolution fusion | flops 1477181440 | bytes 9179136 | tf_op jit(solution)/shard_map/dot_general | solution.py:47
  217.2 0.0 reduce-scatter.11.cloned.1.call-update
  217.2 0.0 all-gather.5.cloned.1.call-start
  217.3 0.1 fusion.59
  217.4 0.1 fusion.69
  217.5 5.8 %psum.22 = f32[256,1]{0,1:T(1,128)S(1)} all-reduce(f32[256,1]{0,1:T(1,128)S(1)} %bitcast.34), channel_id=1, replica_groups=mesh['grp'=2,'ra'=4,'cb'=4] {'cb'}, use_global_device_ids=true, to_apply=%region_5.6 | all-reduce | flops 256 | bytes 2048 | tf_op jit(solution)/shard_map/psum | solution.py:21
  223.3 23.4 %reduce-scatter.9.cloned.1.call-done = f32[256,704]{0,1:T(8,128)} async-done(((f32[256,2816]{0,1:T(8,128)}), f32[256,704]{0,1:T(8,128)}) %reduce-scatter.9.cloned.1.call-update) | async-done | bytes 720912 | tf_op jit(solution)/shard_map/reduce_scatter | solution.py:51
  246.7 38.6 %reduce-scatter.11.cloned.1.call-done = f32[256,704]{0,1:T(8,128)} async-done(((f32[256,2816]{0,1:T(8,128)}), f32[256,704]{0,1:T(8,128)}) %reduce-scatter.11.cloned.1.call-update) | async-done | bytes 720912 | tf_op jit(solution)/shard_map/reduce_scatter | solution.py:52
  285.3 1.6 multiply_multiply_fusion.2
  286.9 2.2 fusion.34
  289.1 0.0 all-gather.5.cloned.1.call-update
  289.1 19.1 %all-gather.5.cloned.1.call-done = bf16[256,2816]{0,1:T(8,128)(2,1)} async-done(((bf16[256,704]{0,1:T(8,128)(2,1)}), bf16[256,2816]{0,1:T(8,128)(2,1)}) %all-gather.5.cloned.1.call-update) | async-done | bytes 1441808 | tf_op jit(solution)/shard_map/all_gather | solution.py:66
  308.1 4.8 %fusion = f32[256,1024]{1,0:T(8,128)S(1)} fusion(bf16[256,2816]{0,1:T(8,128)(2,1)} %all-gather.5.cloned.1.call-done, bf16[2,2816,1024]{2,1,0:T(8,128)(2,1)} %convert.14), kind=kOutput, calls=%fused_computation.1 | convolution fusion | flops 1476395008 | bytes 8257536 | tf_op jit(solution)/shard_map/dot_general | solution.py:67
  312.9 1.5 collective-permute-start.2
  314.5 23.8 %collective-permute-done.2 = f32[256,1024]{1,0:T(8,128)S(1)} collective-permute-done((f32[256,1024]{1,0:T(8,128)S(1)}, f32[256,1024]{1,0:T(8,128)S(1)}, u32[]{:S(2)}, u32[]{:S(2)}) %collective-permute-start.2) | collective-permute-done | bytes 1048608 | tf_op jit(solution)/shard_map/ppermute | solution.py:73
  338.3 0.2 add.113
  338.4 2.5 collective-permute-start.3
  340.9 45.4 %collective-permute-done.3 = f32[256,1024]{1,0:T(8,128)S(1)} collective-permute-done((f32[256,1024]{1,0:T(8,128)S(1)}, f32[256,1024]{1,0:T(8,128)S(1)}, u32[]{:S(2)}, u32[]{:S(2)}) %collective-permute-start.3) | collective-permute-done | bytes 1048608 | tf_op jit(solution)/shard_map/ppermute | solution.py:73
  386.3 0.4 fusion.6
  386.7 5.8 %psum.23 = f32[256,1]{0,1:T(1,128)S(1)} all-reduce(f32[256,1]{0,1:T(1,128)S(1)} %bitcast.37), channel_id=1, replica_groups=mesh['grp'=2,'ra'=4,'cb'=4] {'cb'}, use_global_device_ids=true, to_apply=%region_9.10 | all-reduce | flops 256 | bytes 2048 | tf_op jit(solution)/shard_map/psum | solution.py:21
  392.4 1.0 fusion.8
  (13 shorter events, 0.1 us)
Async XLA Ops:
  6.5 57.0 %reduce-scatter.5.cloned.1.call-start = ((), (), s32[]{:S(2)}) async-start(), calls=%async_computation.4 | async-start | bytes 3604480 | tf_op jit(solution)/shard_map/reduce_scatter | solution.py:51
  7.4 12.8 %copy-start.2 = (bf16[256,1024]{1,0:T(8,128)(2,1)S(1)}, bf16[256,1024]{1,0:T(8,128)(2,1)}, u32[]{:S(2)}) copy-start(bf16[256,1024]{1,0:T(8,128)(2,1)} %param.10) | copy-start | bytes 1572868
  16.0 4.2 %copy-start.1 = (bf16[2,1024,2816]{2,1,0:T(8,128)(2,1)}, bf16[2,1024,2816]{2,1,0:T(8,128)(2,1)S(1)}, u32[]{:S(2)}) copy-start(bf16[2,1024,2816]{2,1,0:T(8,128)(2,1)S(1)} %convert.12) | copy-start | bytes 34603012
  24.3 78.0 %reduce-scatter.7.cloned.1.call-start = ((), (), s32[]{:S(2)}) async-start(), calls=%async_computation.5 | async-start | bytes 3604480 | tf_op jit(solution)/shard_map/reduce_scatter | solution.py:52
  32.9 4.8 %copy-start = (bf16[2,1024,2816]{2,1,0:T(8,128)(2,1)}, bf16[2,1024,2816]{2,1,0:T(8,128)(2,1)S(1)}, u32[]{:S(2)}) copy-start(bf16[2,1024,2816]{2,1,0:T(8,128)(2,1)S(1)} %convert.13) | copy-start | bytes 34603012
  37.7 4.1 %copy-start.5 = (f32[2,2816]{1,0:T(2,128)S(1)}, f32[2,2816]{1,0:T(2,128)}, u32[]{:S(2)}) copy-start(f32[2,2816]{1,0:T(2,128)} %param.14) | copy-start | bytes 67588
  37.8 4.1 %copy-start.6 = (f32[2,2816]{1,0:T(2,128)S(1)}, f32[2,2816]{1,0:T(2,128)}, u32[]{:S(2)}) copy-start(f32[2,2816]{1,0:T(2,128)} %param.15) | copy-start | bytes 67588
  37.8 13.5 %copy-start.3 = (f32[2,3,2816]{2,0,1:T(2,128)S(1)}, f32[2,3,2816]{2,0,1:T(2,128)}, u32[]{:S(2)}) copy-start(f32[2,3,2816]{2,0,1:T(2,128)} %param.16) | copy-start | bytes 202756
  37.8 13.5 %copy-start.4 = (f32[2,3,2816]{2,0,1:T(2,128)S(1)}, f32[2,3,2816]{2,0,1:T(2,128)}, u32[]{:S(2)}) copy-start(f32[2,3,2816]{2,0,1:T(2,128)} %param.17) | copy-start | bytes 202756
  41.8 83.4 %all-gather.3.cloned.1.call-start = ((), (), s32[]{:S(2)}) async-start(), calls=%async_computation.6 | async-start | bytes 1802240 | tf_op jit(solution)/shard_map/all_gather | solution.py:66
  106.1 140.5 %reduce-scatter.9.cloned.1.call-start = ((), (), s32[]{:S(2)}) async-start(), calls=%async_computation.7 | async-start | bytes 3604480 | tf_op jit(solution)/shard_map/reduce_scatter | solution.py:51
  118.8 39.2 %copy-start.7 = (f32[2,1024]{1,0:T(2,128)S(1)}, f32[2,1024]{1,0:T(2,128)}, u32[]{:S(2)}) copy-start(f32[2,1024]{1,0:T(2,128)} %param.19) | copy-start | bytes 24580
  129.9 25.4 %collective-permute-start = (f32[256,1024]{1,0:T(8,128)S(1)}, f32[256,1024]{1,0:T(8,128)S(1)}, u32[]{:S(2)}, u32[]{:S(2)}) collective-permute-start(f32[256,1024]{1,0:T(8,128)S(1)} %fusion.3), channel_id=1, source_target_pairs={{0,4},{4,0},{8,12},{12,8},{1,5},{5,1},{9,13},{13,9},{2,6},{6,2},{1... | collective-permute-start | bytes 3145736 | tf_op jit(solution)/shard_map/ppermute | solution.py:73
  155.5 47.9 %collective-permute-start.1 = (f32[256,1024]{1,0:T(8,128)S(1)}, f32[256,1024]{1,0:T(8,128)S(1)}, u32[]{:S(2)}, u32[]{:S(2)}) collective-permute-start(f32[256,1024]{1,0:T(8,128)S(1)} %add.103), channel_id=1, source_target_pairs={{0,8},{4,12},{8,0},{12,4},{1,9},{5,13},{9,1},{13,5},{2,10},{6,14},... | collective-permute-start | bytes 3145736 | tf_op jit(solution)/shard_map/ppermute | solution.py:73
  210.3 75.0 %reduce-scatter.11.cloned.1.call-start = ((), (), s32[]{:S(2)}) async-start(), calls=%async_computation.8 | async-start | bytes 3604480 | tf_op jit(solution)/shard_map/reduce_scatter | solution.py:52
  217.2 90.9 %all-gather.5.cloned.1.call-start = ((), (), s32[]{:S(2)}) async-start(), calls=%async_computation.9 | async-start | bytes 1802240 | tf_op jit(solution)/shard_map/all_gather | solution.py:66
  312.9 25.4 %collective-permute-start.2 = (f32[256,1024]{1,0:T(8,128)S(1)}, f32[256,1024]{1,0:T(8,128)S(1)}, u32[]{:S(2)}, u32[]{:S(2)}) collective-permute-start(f32[256,1024]{1,0:T(8,128)S(1)} %fusion), channel_id=1, source_target_pairs={{0,4},{4,0},{8,12},{12,8},{1,5},{5,1},{9,13},{13,9},{2,6},{6,2},{1... | collective-permute-start | bytes 3145736 | tf_op jit(solution)/shard_map/ppermute | solution.py:73
  338.4 47.9 %collective-permute-start.3 = (f32[256,1024]{1,0:T(8,128)S(1)}, f32[256,1024]{1,0:T(8,128)S(1)}, u32[]{:S(2)}, u32[]{:S(2)}) collective-permute-start(f32[256,1024]{1,0:T(8,128)S(1)} %add.113), channel_id=1, source_target_pairs={{0,8},{4,12},{8,0},{12,4},{1,9},{5,13},{9,1},{13,5},{2,10},{6,14},... | collective-permute-start | bytes 3145736 | tf_op jit(solution)/shard_map/ppermute | solution.py:73
Sparse Core Ops, SparseCore 0:
  24.4 39.0 reduce-scatter.4
  66.1 36.1 reduce-scatter.6
  106.2 18.8 all-gather.2
  210.4 36.1 reduce-scatter.8
  249.0 36.1 reduce-scatter.10
  289.2 18.8 all-gather.4
